TPU v7x, 256 devices: a whole 4x4x8 slice. The times are simulated.
256 devices in a mesh: sp: 64 (over z, x, core), tp: 4 (over y).
Axes of the slice: x: 4, y: 4, z: 8, core: 2. Of those that a mesh axis runs over, the one named last changes fastest.
Arguments:
- inputs: bfloat16 [32768, 2048], P('sp', 'tp'), may hold values from -45 to 45
- norm_gain: float32 [3, 2048], replicated, may hold values from 0.1 to 1.9
- w_value: bfloat16 [3, 2048, 1024], P(None, 'sp', 'tp'), may hold values from -0.125 to 0.125
- w_gate: bfloat16 [3, 2048, 1024], P(None, 'sp', 'tp'), may hold values from -0.125 to 0.125
- conv_taps: float32 [3, 31, 1024], P(None, None, 'tp'), may hold values from -5 to 5
- ln_gain: float32 [3, 1024], P(None, 'tp'), may hold values from 0.1 to 1.9
- ln_bias: float32 [3, 1024], P(None, 'tp'), may hold values from -3 to 3
- w_out: bfloat16 [3, 1024, 2048], P(None, 'tp', 'sp'), may hold values from -0.1875 to 0.1875
Outputs:
- stream: bfloat16 [32768, 2048], P('sp', 'tp')
All inputs are finite; a program needn't handle non-finite values.
Results may differ from a plain program's by a relative error of at most 0.01.
Values may be sent and summed in bfloat16 or wider, within the bound.
No kernel may reach another device: no remote copies, remote signals or barrier semaphores. Data moves between devices by JAX's collectives and lax.ppermute only.
A program may use at most 64 MiB of HBM per device.

v0:
```python
import jax
import jax.numpy as jnp
from jax import lax
from jax.sharding import PartitionSpec as P


def turned_gather(arrays, axis, dims):
    turned = [jnp.moveaxis(a, dim, 0) for a, dim in zip(arrays, dims)]
    both = jnp.concatenate([t.reshape(len(t), -1) for t in turned], axis=1)
    out, at, gathered = (lax.all_gather(both, axis, axis=0, tiled=True), 0, [])
    for t, dim in zip(turned, dims):
        piece = out[:, at : at + t[0].size].reshape(-1, *t.shape[1:])
        gathered.append(jnp.moveaxis(piece, 0, dim))
        at += t[0].size
    return tuple(gathered)


def laid_out(blocks, dim):
    blocks = jnp.moveaxis(blocks, 0, dim)
    dims = blocks.shape
    return blocks.reshape(*dims[:dim], dims[dim] * dims[dim + 1], *dims[dim + 2 :])


def copy_for_each(array, axis):
    count = lax.axis_size(axis)
    return lax.all_to_all(
        jnp.broadcast_to(array[None], (count, *array.shape)), axis, 0, 0, tiled=True
    )


def collect(array, axis, dim):
    return laid_out(copy_for_each(array, axis), dim)


def from_behind(block, axis, distance):
    devices = range(lax.axis_size(axis))
    route = [(i - distance, i) for i in devices if i - distance in devices]
    return lax.ppermute(block, axis, route)


def taken_together(array, axis):
    return copy_for_each(array, axis).sum(axis=0)


def packed_total(arrays, axis):
    ends = [0]
    for a in arrays:
        ends.append(ends[-1] + a.size)
    so_far = taken_together(jnp.concatenate([a.ravel() for a in arrays]), axis)
    return tuple((so_far[b:e].reshape(a.shape) for a, b, e in zip(arrays, ends, ends[1:])))


def cut_along(array, dim, count):
    dims = array.shape
    blocks = array.reshape(*dims[:dim], count, dims[dim] // count, *dims[dim + 1 :])
    return jnp.moveaxis(blocks, dim, 0)


def sent_and_summed(array, axis, dim):
    count = lax.axis_size(axis)
    blocks = lax.all_to_all(cut_along(array, dim, count), axis, 0, 0, tiled=True)
    return jnp.sum(blocks.astype(jnp.float32), axis=0)


def shards(inputs, norm_gain, w_value, w_gate, conv_taps, ln_gain, ln_bias, w_out):
    rows = inputs.shape[0]
    reach = conv_taps.shape[1] - 1
    layers = conv_taps.shape[0]
    channels = conv_taps.shape[2] * lax.axis_size("tp")
    whole_value, whole_gate, whole_out = turned_gather((w_value, w_gate, w_out), "sp", (1, 1, 2))
    stream = inputs
    for layer in range(layers):
        full_rows = collect(stream, "tp", 1)
        xf = full_rows.astype(jnp.float32)
        meansq = jnp.mean(xf * xf, axis=1, keepdims=True)
        hidden = (xf * lax.rsqrt(meansq + 1e-06) * norm_gain[layer][None, :]).astype(jnp.bfloat16)
        value = jnp.dot(hidden, whole_value[layer], preferred_element_type=jnp.float32)
        gate = jnp.dot(hidden, whole_gate[layer], preferred_element_type=jnp.float32)
        glu = (value * jax.nn.sigmoid(gate)).astype(jnp.bfloat16)
        rim = from_behind(glu[rows - reach :], "sp", 1)
        padded = jnp.concatenate([rim, glu], axis=0)
        count = padded.shape[0] - reach
        filtered = jnp.zeros((count, glu.shape[1]), jnp.float32)
        for tap in range(reach + 1):
            filtered = filtered + conv_taps[layer, tap][None, :] * padded[tap : tap + count].astype(
                jnp.float32
            )
        total_sum, total_sq = packed_total(
            (jnp.sum(filtered, axis=1), jnp.sum(filtered * filtered, axis=1)), "tp"
        )
        mean_val = (total_sum / channels)[:, None]
        var_val = (total_sq / channels)[:, None] - mean_val * mean_val
        normed = jax.nn.silu(
            (filtered - mean_val) * lax.rsqrt(var_val + 1e-06) * ln_gain[layer][None, :]
            + ln_bias[layer][None, :]
        ).astype(jnp.bfloat16)
        partial_out = jnp.dot(normed, whole_out[layer], preferred_element_type=jnp.float32)
        summed = sent_and_summed(partial_out.astype(jnp.bfloat16), "tp", 1)
        kept = stream.astype(jnp.float32)
        stream = (kept + summed).astype(jnp.bfloat16)
    return stream


def solution(mesh):
    in_specs = (
        P("sp", "tp"),
        P(),
        P(None, "sp", "tp"),
        P(None, "sp", "tp"),
        P(None, None, "tp"),
        P(None, "tp"),
        P(None, "tp"),
        P(None, "tp", "sp"),
    )
    out_specs = P("sp", "tp")
    return jax.shard_map(shards, mesh=mesh, in_specs=in_specs, out_specs=out_specs, check_vma=False)
```

profile of v0, /device:TPU:4, one launch (start us, length us, event | category | flops | bytes accessed | tf_op | source)
XLA Modules:
  0.0 334.8 jit_solution(13739559751142840529)
XLA Ops:
  6.5 0.8 copy.95
  7.3 0.8 copy.94
  8.1 0.8 copy.93
  8.9 0.7 pad_maximum_fusion.3
  9.6 1.3 copy.60
  10.9 1.5 broadcast_in_dim.12
  12.4 4.5 %all-to-all-start = ((bf16[4,512,512]{1,2,0:T(8,128)(2,1)}), bf16[4,512,512]{1,2,0:T(8,128)(2,1)S(1)}, u32[]{:S(2)}, u32[]{:S(2)}) async-start(bf16[4,512,512]{1,2,0:T(8,128)(2,1)} %broadcast_in_dim.12), calls=%async_computation | async-start | bytes 4194304 | tf_op jit(solution)/shard_map/all_to_all | solution.py:26
  17.0 26.2 %all-to-all-done = bf16[4,512,512]{1,2,0:T(8,128)(2,1)S(1)} async-done(((bf16[4,512,512]{1,2,0:T(8,128)(2,1)}), bf16[4,512,512]{1,2,0:T(8,128)(2,1)S(1)}, u32[]{:S(2)}, u32[]{:S(2)}) %all-to-all-start) | async-done | bytes 2097184 | tf_op jit(solution)/shard_map/all_to_all | solution.py:26
  43.7 1.9 fusion.2
  45.6 50.0 %all-gather.2.cloned.1.call-done = bf16[2048,2304]{1,0:T(8,128)(2,1)} async-done(((bf16[32,2304]{1,0:T(8,128)(2,1)}), bf16[2048,2304]{1,0:T(8,128)(2,1)}) %all-gather.2.cloned.1.call-update) | async-done | bytes 9437200 | tf_op jit(solution)/shard_map/all_gather | solution.py:10
  95.6 6.1 %fusion.129 = (bf16[2048,768]{1,0:T(8,128)(2,1)}, bf16[2048,768]{1,0:T(8,128)(2,1)S(1)}, bf16[2048,768]{1,0:T(8,128)(2,1)}) fusion(bf16[2048,2304]{1,0:T(8,128)(2,1)} %all-gather.2.cloned.1.call-done), kind=kLoop, calls=%fused_computation.292 | loop fusion | bytes 18874368 | tf_op jit(solution)/shard_map/slice | solution.py:12
  101.6 4.8 %copy.66 = bf16[2048,768]{0,1:T(8,128)(2,1)} copy(bf16[2048,768]{1,0:T(8,128)(2,1)} %get-tuple-element.19) | data formatting | bytes 6291456 | tf_op jit(solution)/shard_map/slice | solution.py:12
  106.4 4.7 %copy.64 = bf16[2048,768]{0,1:T(8,128)(2,1)} copy(bf16[2048,768]{1,0:T(8,128)(2,1)} %get-tuple-element.17) | data formatting | bytes 6291456 | tf_op jit(solution)/shard_map/slice | solution.py:12
  111.1 2.8 fusion.17
  113.9 2.0 fusion.18
  115.9 2.2 collective-permute-start
  118.1 2.9 collective-permute-done
  121.0 3.0 fusion.128
  124.0 0.6 broadcast_in_dim.13
  124.6 4.3 %all-to-all-start.1 = ((f32[4,1,1024]{2,1,0:T(1,128)}), f32[4,1,1024]{2,1,0:T(1,128)S(1)}, u32[]{:S(2)}, u32[]{:S(2)}) async-start(f32[4,1,1024]{2,1,0:T(1,128)} %broadcast_in_dim.13), calls=%async_computation.1 | async-start | bytes 32768 | tf_op jit(solution)/shard_map/all_to_all | solution.py:26
  128.9 3.0 copy.69
  131.9 2.4 all-to-all-done.1
  134.3 2.2 convolution_convert_fusion.2
  136.7 27.0 %all_to_all.48 = bf16[4,512,512]{2,1,0:T(8,128)(2,1)S(1)} all-to-all(bf16[4,512,512]{2,1,0:T(8,128)(2,1)S(1)} %bitcast.186), channel_id=1, replica_groups=mesh['sp'=64,'tp'=4] {'tp'}, dimensions={0} | all-to-all | bytes 4194304 | tf_op jit(solution)/shard_map/all_to_all | solution.py:61
  164.4 1.5 broadcast_in_dim.14
  165.9 3.6 %all-to-all-start.3 = ((bf16[4,512,512]{1,2,0:T(8,128)(2,1)}), bf16[4,512,512]{1,2,0:T(8,128)(2,1)S(1)}, u32[]{:S(2)}, u32[]{:S(2)}) async-start(bf16[4,512,512]{1,2,0:T(8,128)(2,1)} %broadcast_in_dim.14), calls=%async_computation.3 | async-start | bytes 4194304 | tf_op jit(solution)/shard_map/all_to_all | solution.py:26
  169.6 23.2 %all-to-all-done.3 = bf16[4,512,512]{1,2,0:T(8,128)(2,1)S(1)} async-done(((bf16[4,512,512]{1,2,0:T(8,128)(2,1)}), bf16[4,512,512]{1,2,0:T(8,128)(2,1)S(1)}, u32[]{:S(2)}, u32[]{:S(2)}) %all-to-all-start.3) | async-done | bytes 2097184 | tf_op jit(solution)/shard_map/all_to_all | solution.py:26
  193.8 2.0 fusion.14
  195.8 2.0 fusion.19
  197.8 2.1 collective-permute-start.1
  200.0 2.9 collective-permute-done.1
  202.9 2.4 fusion.127
  205.4 7.7 %all_to_all.49 = f32[4,1,1024]{2,1,0:T(1,128)S(1)} all-to-all(f32[4,1,1024]{2,1,0:T(1,128)S(1)} %broadcast_in_dim.15), channel_id=1, replica_groups=mesh['sp'=64,'tp'=4] {'tp'}, dimensions={0} | all-to-all | bytes 32768 | tf_op jit(solution)/shard_map/all_to_all | solution.py:26
  213.1 2.0 convolution_convert_fusion.1
  215.3 29.3 %all_to_all.50 = bf16[4,512,512]{2,1,0:T(8,128)(2,1)S(1)} all-to-all(bf16[4,512,512]{2,1,0:T(8,128)(2,1)S(1)} %bitcast.187), channel_id=1, replica_groups=mesh['sp'=64,'tp'=4] {'tp'}, dimensions={0} | all-to-all | bytes 4194304 | tf_op jit(solution)/shard_map/all_to_all | solution.py:61
  245.4 1.5 broadcast_in_dim.16
  246.9 3.6 %all-to-all-start.6 = ((bf16[4,512,512]{1,2,0:T(8,128)(2,1)}), bf16[4,512,512]{1,2,0:T(8,128)(2,1)S(1)}, u32[]{:S(2)}, u32[]{:S(2)}) async-start(bf16[4,512,512]{1,2,0:T(8,128)(2,1)} %broadcast_in_dim.16), calls=%async_computation.6 | async-start | bytes 4194304 | tf_op jit(solution)/shard_map/all_to_all | solution.py:26
  250.5 27.4 %all-to-all-done.6 = bf16[4,512,512]{1,2,0:T(8,128)(2,1)S(1)} async-done(((bf16[4,512,512]{1,2,0:T(8,128)(2,1)}), bf16[4,512,512]{1,2,0:T(8,128)(2,1)S(1)}, u32[]{:S(2)}, u32[]{:S(2)}) %all-to-all-start.6) | async-done | bytes 2097184 | tf_op jit(solution)/shard_map/all_to_all | solution.py:26
  278.4 0.5 fusion.8
  279.0 2.0 fusion.11
  281.0 2.0 fusion.20
  283.0 1.9 collective-permute-start.2
  285.0 3.1 collective-permute-done.2
  288.1 2.4 fusion.126
  290.5 7.7 %all_to_all.51 = f32[4,1,1024]{2,1,0:T(1,128)S(1)} all-to-all(f32[4,1,1024]{2,1,0:T(1,128)S(1)} %broadcast_in_dim.17), channel_id=1, replica_groups=mesh['sp'=64,'tp'=4] {'tp'}, dimensions={0} | all-to-all | bytes 32768 | tf_op jit(solution)/shard_map/all_to_all | solution.py:26
  298.3 2.0 convolution_convert_fusion
  300.5 26.1 %all_to_all.52 = bf16[4,512,512]{2,1,0:T(8,128)(2,1)S(1)} all-to-all(bf16[4,512,512]{2,1,0:T(8,128)(2,1)S(1)} %bitcast.188), channel_id=1, replica_groups=mesh['sp'=64,'tp'=4] {'tp'}, dimensions={0} | all-to-all | bytes 4194304 | tf_op jit(solution)/shard_map/all_to_all | solution.py:61
  327.0 1.0 add_convert_fusion
  (56 shorter events, 4.8 us)
Async XLA Ops:
  6.5 89.0 %all-gather.2.cloned.1.call-start = ((), (), s32[]{:S(2)}) async-start(), calls=%async_computation.9 | async-start | bytes 9584640 | tf_op jit(solution)/shard_map/all_gather | solution.py:10
  10.9 6.0 %copy-start.3 = (f32[3,2048]{1,0:T(4,128)S(1)}, f32[3,2048]{1,0:T(4,128)}, u32[]{:S(2)}) copy-start(f32[3,2048]{1,0:T(4,128)} %param.9) | copy-start | bytes 73732
  10.9 6.0 %copy-start.2 = (f32[3,31,256]{2,1,0:T(8,128)S(1)}, f32[3,31,256]{2,1,0:T(8,128)}, u32[]{:S(2)}) copy-start(f32[3,31,256]{2,1,0:T(8,128)} %param.12) | copy-start | bytes 285700
  12.4 30.8 %all-to-all-start = ((bf16[4,512,512]{1,2,0:T(8,128)(2,1)}), bf16[4,512,512]{1,2,0:T(8,128)(2,1)S(1)}, u32[]{:S(2)}, u32[]{:S(2)}) async-start(bf16[4,512,512]{1,2,0:T(8,128)(2,1)} %broadcast_in_dim.12), calls=%async_computation | async-start | bytes 4194304 | tf_op jit(solution)/shard_map/all_to_all | solution.py:26
  111.1 2.8 copy-start
  113.9 4.2 %copy-start.4 = (f32[3,256]{1,0:T(4,128)S(1)}, f32[3,256]{1,0:T(4,128)}, u32[]{:S(2)}) copy-start(f32[3,256]{1,0:T(4,128)} %param.14) | copy-start | bytes 9220
  113.9 15.0 %copy-start.5 = (f32[3,256]{1,0:T(4,128)S(1)}, f32[3,256]{1,0:T(4,128)}, u32[]{:S(2)}) copy-start(f32[3,256]{1,0:T(4,128)} %param.13) | copy-start | bytes 9220
  115.9 5.1 %collective-permute-start = (bf16[30,256]{1,0:T(8,128)(2,1)S(1)}, bf16[30,256]{1,0:T(8,128)(2,1)S(1)}, u32[]{:S(2)}, u32[]{:S(2)}) collective-permute-start(bf16[30,256]{1,0:T(8,128)(2,1)S(1)} %slice.856), channel_id=1, source_target_pairs={{0,4},{4,8},{8,12},{12,16},{16,20},{20,24},{24,28},{28,32},{32,36}... | collective-permute-start | bytes 46088 | tf_op jit(solution)/shard_map/ppermute | solution.py:38
  124.6 9.6 %all-to-all-start.1 = ((f32[4,1,1024]{2,1,0:T(1,128)}), f32[4,1,1024]{2,1,0:T(1,128)S(1)}, u32[]{:S(2)}, u32[]{:S(2)}) async-start(f32[4,1,1024]{2,1,0:T(1,128)} %broadcast_in_dim.13), calls=%async_computation.1 | async-start | bytes 32768 | tf_op jit(solution)/shard_map/all_to_all | solution.py:26
  136.7 27.3 %copy-start.1 = (bf16[512,512]{1,0:T(8,128)(2,1)S(1)}, bf16[512,512]{1,0:T(8,128)(2,1)}, u32[]{:S(2)}) copy-start(bf16[512,512]{1,0:T(8,128)(2,1)} %param.8) | copy-start | bytes 1572868
  165.9 26.8 %all-to-all-start.3 = ((bf16[4,512,512]{1,2,0:T(8,128)(2,1)}), bf16[4,512,512]{1,2,0:T(8,128)(2,1)S(1)}, u32[]{:S(2)}, u32[]{:S(2)}) async-start(bf16[4,512,512]{1,2,0:T(8,128)(2,1)} %broadcast_in_dim.14), calls=%async_computation.3 | async-start | bytes 4194304 | tf_op jit(solution)/shard_map/all_to_all | solution.py:26
  197.8 5.1 %collective-permute-start.1 = (bf16[30,256]{1,0:T(8,128)(2,1)S(1)}, bf16[30,256]{1,0:T(8,128)(2,1)S(1)}, u32[]{:S(2)}, u32[]{:S(2)}) collective-permute-start(bf16[30,256]{1,0:T(8,128)(2,1)S(1)} %slice.919), channel_id=1, source_target_pairs={{0,4},{4,8},{8,12},{12,16},{16,20},{20,24},{24,28},{28,32},{32,36}... | collective-permute-start | bytes 46088 | tf_op jit(solution)/shard_map/ppermute | solution.py:38
  246.9 31.1 %all-to-all-start.6 = ((bf16[4,512,512]{1,2,0:T(8,128)(2,1)}), bf16[4,512,512]{1,2,0:T(8,128)(2,1)S(1)}, u32[]{:S(2)}, u32[]{:S(2)}) async-start(bf16[4,512,512]{1,2,0:T(8,128)(2,1)} %broadcast_in_dim.16), calls=%async_computation.6 | async-start | bytes 4194304 | tf_op jit(solution)/shard_map/all_to_all | solution.py:26
  283.0 5.1 %collective-permute-start.2 = (bf16[30,256]{1,0:T(8,128)(2,1)S(1)}, bf16[30,256]{1,0:T(8,128)(2,1)S(1)}, u32[]{:S(2)}, u32[]{:S(2)}) collective-permute-start(bf16[30,256]{1,0:T(8,128)(2,1)S(1)} %slice.981), channel_id=1, source_target_pairs={{0,4},{4,8},{8,12},{12,16},{16,20},{20,24},{24,28},{28,32},{32,36}... | collective-permute-start | bytes 46088 | tf_op jit(solution)/shard_map/ppermute | solution.py:38
Sparse Core Ops, SparseCore 0:
  10.1 85.4 all-gather.1
where the time goes:
time: 336 us; the launch traced here: 335 us
  waiting for transfers between devices  138 us (41%)
  blocking collectives  97.9 us (29%)
  local copies, waits for them, and re-layouts  28.5 us (8%)
  starting transfers between devices  22.1 us (7%)
  matrix products  19.1 us (6%)
  other arithmetic  15.3 us (5%)
  between operations  13.8 us (4%)
    all_to_all x3, blocking collectives, sent_and_summed(): lax.all_to_all(cut_along(array, dim, count), axis, 0, 0, tiled=True)  82.5 us
    all_to_all x4, waiting for transfers between devices, copy_for_each(): lax.all_to_all(jnp.broadcast_to(array[None], (count, *array.shape)), axis...  79.2 us
    all_gather x1, waiting for transfers between devices, turned_gather(): out, at, gathered = (lax.all_gather(both, axis, axis=0, tiled=True), 0, [])  50 us
    slice x4, local copies, waits for them, and re-layouts, turned_gather(): piece = out[:, at:at + t[0].size].reshape(-1, *t.shape[1:])  18.5 us
    all_to_all x4, starting transfers between devices, copy_for_each(): lax.all_to_all(jnp.broadcast_to(array[None], (count, *array.shape)), axis...  16 us
    all_to_all x2, blocking collectives, copy_for_each(): lax.all_to_all(jnp.broadcast_to(array[None], (count, *array.shape)), axis...  15.4 us
    ppermute x3, waiting for transfers between devices, from_behind(): return lax.ppermute(block, axis, route)  8.89 us
    reduce_sum x3, other arithmetic, shards(): jnp.sum(filtered, axis=1)  7.83 us
  transfers between devices with their start and end apart: 8, of which 8 were waited for; matrix products, arithmetic and copies ran while one was open for 2% of the time, Pallas kernels for 0%

commit v1 on v0

--- a/solution.py
+++ b/solution.py
@@ -4,10 +4,15 @@
 from jax.sharding import PartitionSpec as P
 
 
+def swapped_in(shard, name, along):
+    repeated = jnp.stack([shard] * lax.axis_size(name))
+    return jnp.concatenate(lax.all_to_all(repeated, name, 0, 0), axis=along)
+
+
 def turned_gather(arrays, axis, dims):
     turned = [jnp.moveaxis(a, dim, 0) for a, dim in zip(arrays, dims)]
     both = jnp.concatenate([t.reshape(len(t), -1) for t in turned], axis=1)
-    out, at, gathered = (lax.all_gather(both, axis, axis=0, tiled=True), 0, [])
+    out, at, gathered = (swapped_in(both, axis, 0), 0, [])
     for t, dim in zip(turned, dims):
         piece = out[:, at : at + t[0].size].reshape(-1, *t.shape[1:])
         gathered.append(jnp.moveaxis(piece, 0, dim))

time: 336 us -> 491 us (1.46)
  waiting for transfers between devices: 138 us -> 291 us
  between operations: 13.8 us -> 0.51 us
  starting transfers between devices: 22.1 us -> 34.1 us
    all_to_all x0 -> x1, waiting for transfers between devices: none -> 204 us  [swapped_in(): return jnp.concatenate(lax.all_to_all(repeated, name, 0, 0), axis=along)]
    all_gather x1 -> x0, waiting for transfers between devices: 50 us -> none  [turned_gather(): out, at, gathered = (lax.all_gather(both, axis, axis=0, tiled=True), 0, [])]
    all_to_all x0 -> x1, starting transfers between devices: none -> 12.3 us  [swapped_in(): return jnp.concatenate(lax.all_to_all(repeated, name, 0, 0), axis=along)]
  transfers between devices with their start and end apart: 8 -> 8, of which waited for: 8 -> 8; matrix products, arithmetic and copies ran while one was open for 2% -> 1% of each run, Pallas kernels for 0% -> 0%
where the time goes in v1:
time: 491 us; the launch traced here: 488 us
  waiting for transfers between devices  291 us (59%)
  blocking collectives  97.8 us (20%)
  starting transfers between devices  34.1 us (7%)
  local copies, waits for them, and re-layouts  31 us (6%)
  matrix products  19.1 us (4%)
  other arithmetic  14.7 us (3%)
    all_to_all x1, waiting for transfers between devices, swapped_in(): return jnp.concatenate(lax.all_to_all(repeated, name, 0, 0), axis=along)  204 us
    all_to_all x3, blocking collectives, sent_and_summed(): lax.all_to_all(cut_along(array, dim, count), axis, 0, 0, tiled=True)  82.4 us
    all_to_all x4, waiting for transfers between devices, copy_for_each(): lax.all_to_all(jnp.broadcast_to(array[None], (count, *array.shape)), axis...  78.8 us
    slice x4, local copies, waits for them, and re-layouts, turned_gather(): piece = out[:, at:at + t[0].size].reshape(-1, *t.shape[1:])  18.5 us
    all_to_all x2, blocking collectives, copy_for_each(): lax.all_to_all(jnp.broadcast_to(array[None], (count, *array.shape)), axis...  15.4 us
    all_to_all x4, starting transfers between devices, copy_for_each(): lax.all_to_all(jnp.broadcast_to(array[None], (count, *array.shape)), axis...  15.1 us
    all_to_all x1, starting transfers between devices, swapped_in(): return jnp.concatenate(lax.all_to_all(repeated, name, 0, 0), axis=along)  12.3 us
  transfers between devices with their start and end apart: 8, of which 8 were waited for; matrix products, arithmetic and copies ran while one was open for 1% of the time, Pallas kernels for 0%

profile of v1, /device:TPU:4, one launch (start us, length us, event | category | flops | bytes accessed | tf_op | source)
XLA Modules:
  0.0 488.0 jit_solution(9441938155531404696)
XLA Ops:
  0.0 1.3 copy.73
  1.3 1.5 broadcast_in_dim.12
  2.8 4.5 all-to-all-start
  7.3 26.3 %all-to-all-done = bf16[4,512,512]{1,2,0:T(8,128)(2,1)S(1)} async-done(((bf16[4,512,512]{1,2,0:T(8,128)(2,1)}), bf16[4,512,512]{1,2,0:T(8,128)(2,1)S(1)}, u32[]{:S(2)}, u32[]{:S(2)}) %all-to-all-start) | async-done | bytes 2097184 | tf_op jit(solution)/shard_map/all_to_all | solution.py:31
  33.6 4.8 stack.2
  38.4 12.3 %all-to-all-start.1 = ((bf16[64,32,2304]{2,1,0:T(8,128)(2,1)}), bf16[64,32,2304]{2,1,0:T(8,128)(2,1)}, u32[]{:S(2)}, u32[]{:S(2)}) async-start(bf16[64,32,2304]{2,1,0:T(8,128)(2,1)} %stack.2), calls=%async_computation.1 | async-start | bytes 18874368 | tf_op jit(solution)/shard_map/all_to_all | solution.py:9
  50.9 0.5 fusion
  51.4 1.8 fusion.2
  53.2 203.7 %all-to-all-done.1 = bf16[64,32,2304]{2,1,0:T(8,128)(2,1)} async-done(((bf16[64,32,2304]{2,1,0:T(8,128)(2,1)}), bf16[64,32,2304]{2,1,0:T(8,128)(2,1)}, u32[]{:S(2)}, u32[]{:S(2)}) %all-to-all-start.1) | async-done | bytes 9437216 | tf_op jit(solution)/shard_map/all_to_all | solution.py:9
  256.9 6.1 %fusion.129 = (bf16[2048,768]{1,0:T(8,128)(2,1)}, bf16[2048,768]{1,0:T(8,128)(2,1)S(1)}, bf16[2048,768]{1,0:T(8,128)(2,1)}) fusion(bf16[2048,2304]{1,0:T(8,128)(2,1)} %bitcast.6), kind=kLoop, calls=%fused_computation.292 | loop fusion | bytes 18874368 | tf_op jit(solution)/shard_map/slice | solution.py:17
  263.0 4.8 copy.79
  267.7 4.7 copy.77
  272.4 2.8 fusion.17
  275.3 2.0 fusion.18
  277.3 1.9 collective-permute-start
  279.2 3.1 collective-permute-done
  282.3 3.0 fusion.128
  285.3 0.6 broadcast_in_dim.13
  285.9 3.2 all-to-all-start.2
  289.2 3.0 copy.82
  292.2 2.3 all-to-all-done.2
  294.6 2.2 convolution_convert_fusion.2
  297.0 27.4 %all_to_all.53 = bf16[4,512,512]{2,1,0:T(8,128)(2,1)S(1)} all-to-all(bf16[4,512,512]{2,1,0:T(8,128)(2,1)S(1)} %bitcast.187), channel_id=1, replica_groups=mesh['sp'=64,'tp'=4] {'tp'}, dimensions={0} | all-to-all | bytes 4194304 | tf_op jit(solution)/shard_map/all_to_all | solution.py:66
  325.1 1.5 broadcast_in_dim.14
  326.6 3.8 all-to-all-start.4
  330.4 23.7 %all-to-all-done.4 = bf16[4,512,512]{1,2,0:T(8,128)(2,1)S(1)} async-done(((bf16[4,512,512]{1,2,0:T(8,128)(2,1)}), bf16[4,512,512]{1,2,0:T(8,128)(2,1)S(1)}, u32[]{:S(2)}, u32[]{:S(2)}) %all-to-all-start.4) | async-done | bytes 2097184 | tf_op jit(solution)/shard_map/all_to_all | solution.py:31
  354.6 0.5 fusion.5
  355.2 2.0 fusion.14
  357.2 2.0 fusion.19
  359.2 1.9 collective-permute-start.1
  361.2 3.1 collective-permute-done.1
  364.3 2.4 fusion.127
  366.7 7.7 %all_to_all.54 = f32[4,1,1024]{2,1,0:T(1,128)S(1)} all-to-all(f32[4,1,1024]{2,1,0:T(1,128)S(1)} %broadcast_in_dim.15), channel_id=1, replica_groups=mesh['sp'=64,'tp'=4] {'tp'}, dimensions={0} | all-to-all | bytes 32768 | tf_op jit(solution)/shard_map/all_to_all | solution.py:31
  374.5 2.0 convolution_convert_fusion.1
  376.7 27.9 %all_to_all.55 = bf16[4,512,512]{2,1,0:T(8,128)(2,1)S(1)} all-to-all(bf16[4,512,512]{2,1,0:T(8,128)(2,1)S(1)} %bitcast.188), channel_id=1, replica_groups=mesh['sp'=64,'tp'=4] {'tp'}, dimensions={0} | all-to-all | bytes 4194304 | tf_op jit(solution)/shard_map/all_to_all | solution.py:66
  405.3 1.5 broadcast_in_dim.16
  406.8 3.6 all-to-all-start.7
  410.4 26.5 %all-to-all-done.7 = bf16[4,512,512]{1,2,0:T(8,128)(2,1)S(1)} async-done(((bf16[4,512,512]{1,2,0:T(8,128)(2,1)}), bf16[4,512,512]{1,2,0:T(8,128)(2,1)S(1)}, u32[]{:S(2)}, u32[]{:S(2)}) %all-to-all-start.7) | async-done | bytes 2097184 | tf_op jit(solution)/shard_map/all_to_all | solution.py:31
  437.5 0.5 fusion.8
  438.0 2.0 fusion.11
  440.1 2.0 fusion.20
  442.1 2.9 collective-permute-start.2
  445.0 2.1 collective-permute-done.2
  447.2 2.4 fusion.126
  449.6 7.7 %all_to_all.56 = f32[4,1,1024]{2,1,0:T(1,128)S(1)} all-to-all(f32[4,1,1024]{2,1,0:T(1,128)S(1)} %broadcast_in_dim.17), channel_id=1, replica_groups=mesh['sp'=64,'tp'=4] {'tp'}, dimensions={0} | all-to-all | bytes 32768 | tf_op jit(solution)/shard_map/all_to_all | solution.py:31
  457.4 2.0 convolution_convert_fusion
  459.6 27.1 %all_to_all.57 = bf16[4,512,512]{2,1,0:T(8,128)(2,1)S(1)} all-to-all(bf16[4,512,512]{2,1,0:T(8,128)(2,1)S(1)} %bitcast.189), channel_id=1, replica_groups=mesh['sp'=64,'tp'=4] {'tp'}, dimensions={0} | all-to-all | bytes 4194304 | tf_op jit(solution)/shard_map/all_to_all | solution.py:66
  487.0 1.0 add_convert_fusion
  (62 shorter events, 3.7 us)
Async XLA Ops:
  1.3 6.0 %copy-start.3 = (bf16[3,256,32]{1,2,0:T(8,128)(2,1)S(1)}, bf16[3,256,32]{1,2,0:T(8,128)(2,1)}, u32[]{:S(2)}) copy-start(bf16[3,256,32]{1,2,0:T(8,128)(2,1)} %param.15) | copy-start | bytes 147460
  1.3 6.0 %copy-start.4 = (bf16[3,32,256]{2,1,0:T(8,128)(2,1)S(1)}, bf16[3,32,256]{2,1,0:T(8,128)(2,1)}, u32[]{:S(2)}) copy-start(bf16[3,32,256]{2,1,0:T(8,128)(2,1)} %param.11) | copy-start | bytes 147460
  1.3 6.0 %copy-start.5 = (bf16[3,32,256]{2,1,0:T(8,128)(2,1)S(1)}, bf16[3,32,256]{2,1,0:T(8,128)(2,1)}, u32[]{:S(2)}) copy-start(bf16[3,32,256]{2,1,0:T(8,128)(2,1)} %param.10) | copy-start | bytes 147460
  2.8 30.8 %all-to-all-start = ((bf16[4,512,512]{1,2,0:T(8,128)(2,1)}), bf16[4,512,512]{1,2,0:T(8,128)(2,1)S(1)}, u32[]{:S(2)}, u32[]{:S(2)}) async-start(bf16[4,512,512]{1,2,0:T(8,128)(2,1)} %broadcast_in_dim.12), calls=%async_computation | async-start | bytes 4194304 | tf_op jit(solution)/shard_map/all_to_all | solution.py:31
  38.4 12.3 %copy-start.6 = (f32[3,2048]{1,0:T(4,128)S(1)}, f32[3,2048]{1,0:T(4,128)}, u32[]{:S(2)}) copy-start(f32[3,2048]{1,0:T(4,128)} %param.9) | copy-start | bytes 73732
  38.4 12.4 %copy-start.2 = (f32[3,31,256]{2,1,0:T(8,128)S(1)}, f32[3,31,256]{2,1,0:T(8,128)}, u32[]{:S(2)}) copy-start(f32[3,31,256]{2,1,0:T(8,128)} %param.12) | copy-start | bytes 285700
  38.4 218.5 %all-to-all-start.1 = ((bf16[64,32,2304]{2,1,0:T(8,128)(2,1)}), bf16[64,32,2304]{2,1,0:T(8,128)(2,1)}, u32[]{:S(2)}, u32[]{:S(2)}) async-start(bf16[64,32,2304]{2,1,0:T(8,128)(2,1)} %stack.2), calls=%async_computation.1 | async-start | bytes 18874368 | tf_op jit(solution)/shard_map/all_to_all | solution.py:9
  272.4 2.8 copy-start
  275.2 4.0 copy-start.7
  275.2 14.0 %copy-start.8 = (f32[3,256]{1,0:T(4,128)S(1)}, f32[3,256]{1,0:T(4,128)}, u32[]{:S(2)}) copy-start(f32[3,256]{1,0:T(4,128)} %param.13) | copy-start | bytes 9220
  277.3 5.1 %collective-permute-start = (bf16[30,256]{1,0:T(8,128)(2,1)S(1)}, bf16[30,256]{1,0:T(8,128)(2,1)S(1)}, u32[]{:S(2)}, u32[]{:S(2)}) collective-permute-start(bf16[30,256]{1,0:T(8,128)(2,1)S(1)} %slice.856), channel_id=1, source_target_pairs={{0,4},{4,8},{8,12},{12,16},{16,20},{20,24},{24,28},{28,32},{32,36}... | collective-permute-start | bytes 46088 | tf_op jit(solution)/shard_map/ppermute | solution.py:43
  285.9 8.6 %all-to-all-start.2 = ((f32[4,1,1024]{2,1,0:T(1,128)}), f32[4,1,1024]{2,1,0:T(1,128)S(1)}, u32[]{:S(2)}, u32[]{:S(2)}) async-start(f32[4,1,1024]{2,1,0:T(1,128)} %broadcast_in_dim.13), calls=%async_computation.2 | async-start | bytes 32768 | tf_op jit(solution)/shard_map/all_to_all | solution.py:31
  297.0 27.7 %copy-start.1 = (bf16[512,512]{1,0:T(8,128)(2,1)S(1)}, bf16[512,512]{1,0:T(8,128)(2,1)}, u32[]{:S(2)}) copy-start(bf16[512,512]{1,0:T(8,128)(2,1)} %param.8) | copy-start | bytes 1572868
  326.6 27.5 %all-to-all-start.4 = ((bf16[4,512,512]{1,2,0:T(8,128)(2,1)}), bf16[4,512,512]{1,2,0:T(8,128)(2,1)S(1)}, u32[]{:S(2)}, u32[]{:S(2)}) async-start(bf16[4,512,512]{1,2,0:T(8,128)(2,1)} %broadcast_in_dim.14), calls=%async_computation.4 | async-start | bytes 4194304 | tf_op jit(solution)/shard_map/all_to_all | solution.py:31
  359.2 5.1 %collective-permute-start.1 = (bf16[30,256]{1,0:T(8,128)(2,1)S(1)}, bf16[30,256]{1,0:T(8,128)(2,1)S(1)}, u32[]{:S(2)}, u32[]{:S(2)}) collective-permute-start(bf16[30,256]{1,0:T(8,128)(2,1)S(1)} %slice.919), channel_id=1, source_target_pairs={{0,4},{4,8},{8,12},{12,16},{16,20},{20,24},{24,28},{28,32},{32,36}... | collective-permute-start | bytes 46088 | tf_op jit(solution)/shard_map/ppermute | solution.py:43
  406.8 30.2 %all-to-all-start.7 = ((bf16[4,512,512]{1,2,0:T(8,128)(2,1)}), bf16[4,512,512]{1,2,0:T(8,128)(2,1)S(1)}, u32[]{:S(2)}, u32[]{:S(2)}) async-start(bf16[4,512,512]{1,2,0:T(8,128)(2,1)} %broadcast_in_dim.16), calls=%async_computation.7 | async-start | bytes 4194304 | tf_op jit(solution)/shard_map/all_to_all | solution.py:31
  442.1 5.1 %collective-permute-start.2 = (bf16[30,256]{1,0:T(8,128)(2,1)S(1)}, bf16[30,256]{1,0:T(8,128)(2,1)S(1)}, u32[]{:S(2)}, u32[]{:S(2)}) collective-permute-start(bf16[30,256]{1,0:T(8,128)(2,1)S(1)} %slice.981), channel_id=1, source_target_pairs={{0,4},{4,8},{8,12},{12,16},{16,20},{20,24},{24,28},{28,32},{32,36}... | collective-permute-start | bytes 46088 | tf_op jit(solution)/shard_map/ppermute | solution.py:43
